TPU v7x, 256 devices: a 2x2x32 block of a 4x8x32 slice. The times are simulated.
256 devices in a mesh: grp: 4 (over y, x), ep: 32 (over z), tp: 2 (over core).
Axes of the slice: x: 2, y: 2, z: 32, core: 2. Of those that a mesh axis runs over, the one named last changes fastest.
The devices are a block of a 4x8x32 slice.
Arguments:
- tokens: bfloat16 [16384, 4096], P(('grp', 'ep')), parts along dimension 0, may hold values from -16 to 16, as said below
- norm_gain: float32 [4096], replicated, may hold values from 0.1 to 1.9
- gate_weight: bfloat16 [32, 4096, 768], P('ep', None, 'tp'), may hold values from -0.09375 to 0.09375
- up_weight: bfloat16 [32, 4096, 768], P('ep', None, 'tp'), may hold values from -0.09375 to 0.09375
- down_weight: bfloat16 [32, 768, 4096], P('ep', 'tp'), may hold values from -0.21875 to 0.21875
- chosen: int32 [128, 32, 20], P(('grp', 'ep')), parts along dimension 0, may hold values from 0 to 128, as said below
- affinity: float32 [128, 32, 20], P(('grp', 'ep')), parts along dimension 0, may hold values from 0.2 to 1
Outputs:
- mixed: bfloat16 [16384, 4096], P(('grp', 'ep'), 'tp'), parts along dimension 0
There are 4 independent parts, one for each index of `grp`. A program takes and returns all parts, laid end to end along the dimension named above; an argument that names none is the same for every part. Nothing has to cross between parts.
Inputs may be any that keep to these rules, and one draw needn't show every extreme that they name: `tokens`: draws differ in their scale from row to row. `chosen`: in each (block, expert) row the live entries come first and are distinct; dead entries equal 128. Every expert has exactly 512 live slots in all and at least one live slot in every block; some block gives some expert exactly 20 live slots.
All inputs are finite; a program needn't handle non-finite values.
Results may differ from a plain program's by a relative error of at most 0.0095.
Values may be sent and summed in bfloat16 or wider, within the bound.
A program may use at most 64 MiB of HBM per device.

v0:
```python
import jax
import jax.numpy as jnp
from jax import lax
from jax.sharding import PartitionSpec as P

norm_eps = 1e-06


def cut_along(shard, dim, size):
    before, after = (shard.shape[:dim], shard.shape[dim + 1 :])
    return jnp.moveaxis(shard.reshape(*before, size, -1, *after), dim, 0)


def summed_on_arrival(shard, axis, dim):
    size = lax.axis_size(axis)
    pieces = lax.all_to_all(cut_along(shard, dim, size), axis, 0, 0, tiled=True)
    return jnp.sum(pieces.astype(jnp.float32), axis=0)


def normalize(block, norm_gain):
    values = block.astype(jnp.float32)
    scaled = values * lax.rsqrt(jnp.mean(values * values, axis=-1, keepdims=True) + norm_eps)
    return (scaled * norm_gain).astype(jnp.bfloat16)


def shards(tokens, norm_gain, gate_weight, up_weight, down_weight, chosen, affinity):
    tok_rows = tokens.shape[0]
    model_width = tokens.shape[1]
    slot_count = chosen.shape[2]
    picked_rows = chosen[0]
    source = normalize(tokens, norm_gain)
    half_slots = slot_count // 2
    own_slots = lax.dynamic_slice_in_dim(
        picked_rows, lax.axis_index("tp") * half_slots, half_slots, 1
    )
    outgoing = jnp.take(source, own_slots, axis=0, mode="clip")
    landed = lax.all_to_all(outgoing, "ep", split_axis=0, concat_axis=0, tiled=True)
    arrived = lax.all_gather(landed, "tp", axis=1, tiled=True)
    arrived_rows = arrived.reshape(-1, model_width)
    gate_proj = jnp.dot(arrived_rows, gate_weight[0], preferred_element_type=jnp.float32)
    up_value = jnp.dot(arrived_rows, up_weight[0], preferred_element_type=jnp.float32)
    hidden = (jax.nn.silu(gate_proj) * up_value).astype(jnp.bfloat16)
    columns = down_weight[0]
    summed = summed_on_arrival(
        lax.dot_general(
            columns, hidden, (((0,), (1,)), ((), ())), preferred_element_type=jnp.float32
        ).astype(jnp.bfloat16),
        "tp",
        0,
    )
    expert_out = summed.astype(jnp.bfloat16)
    returned = lax.all_to_all(expert_out, "ep", split_axis=1, concat_axis=1, tiled=True)
    weight = jnp.where(picked_rows < tok_rows, affinity[0], 0.0).astype(jnp.bfloat16).reshape(-1)
    flat_picks = picked_rows.reshape(-1)
    matches = flat_picks[None, :] == jnp.arange(tok_rows, dtype=jnp.int32)[:, None]
    combine = jnp.where(matches, weight[None, :], jnp.zeros((), jnp.bfloat16))
    mixed = lax.dot_general(
        combine, returned, (((1,), (1,)), ((), ())), preferred_element_type=jnp.float32
    )
    return mixed.astype(jnp.bfloat16)


def solution(mesh):
    in_specs = (
        P(("grp", "ep"), None),
        P(),
        P("ep", None, "tp"),
        P("ep", None, "tp"),
        P("ep", "tp", None),
        P(("grp", "ep"), None, None),
        P(("grp", "ep"), None, None),
    )
    out_specs = P(("grp", "ep"), "tp")
    return jax.shard_map(shards, mesh=mesh, in_specs=in_specs, out_specs=out_specs, check_vma=False)
```

profile of v0, /device:TPU:357, one launch (start us, length us, event | category | flops | bytes accessed | tf_op | source)
XLA Modules:
  0.0 832.0 jit_solution(3953942204151701795)
XLA Ops:
  6.5 0.0 copy-start
  6.6 0.0 all-gather.2.cloned.1.call-start
  6.6 0.8 constant_dynamic-slice_fusion
  7.4 0.1 copy.13
  7.5 0.1 reshape.35
  7.6 1.5 fusion.5
  9.1 2.5 fusion.7
  11.7 9.4 %gather_fusion = bf16[320,4096]{1,0:T(8,128)(2,1)} fusion(bf16[128,4096]{1,0:T(8,128)(2,1)} %fusion.7, s32[1024]{0:T(1024)S(1)} %pad_clamp_fusion), kind=kCustom, calls=%fused_computation | custom fusion | bytes 5244160 | tf_op jit(solution)/shard_map/jit(_take)/gather | solution.py:36
  21.1 4.6 reshape.34
  25.7 396.9 %all_to_all.22 = bf16[32,10,4096]{2,1,0:T(8,128)(2,1)S(1)} all-to-all(bf16[32,10,4096]{2,1,0:T(8,128)(2,1)} %reshape.34), channel_id=1, replica_groups=mesh['grp'=4,'ep'=32,'tp'=2] {'ep'}, dimensions={0} | all-to-all | bytes 5242880 | tf_op jit(solution)/shard_map/all_to_all | solution.py:37
  422.6 2.9 copy.14
  425.5 0.1 all-gather.2.cloned.1.call-update
  425.6 26.6 %all-gather.2.cloned.1.call-done = bf16[32,20,4096]{2,0,1:T(8,128)(2,1)} async-done(((bf16[32,10,4096]{2,0,1:T(8,128)(2,1)}), bf16[32,20,4096]{2,0,1:T(8,128)(2,1)}) %all-gather.2.cloned.1.call-update) | async-done | bytes 5242896 | tf_op jit(solution)/shard_map/all_gather | solution.py:38
  452.2 8.1 copy.15
  460.3 7.8 reshape.31
  468.1 7.3 fusion.3
  475.4 0.0 copy-done
  475.4 11.6 %convolution_convert_fusion = bf16[640,4096]{1,0:T(8,128)(2,1)} fusion(bf16[1,384,4096]{2,1,0:T(8,128)(2,1)S(1)} %copy-done, bf16[640,4096]{1,0:T(8,128)(2,1)} %reshape.31, bf16[1,4096,384]{2,1,0:T(8,128)(2,1)} %param.10, f32[640,384]{1,0:T(8,128)} %fusion.3), kind=kOutput, calls=%fused_computation.1 | convolution fusion | flops 4030627840 | bytes 17760256 | tf_op jit(solution)/shard_map/dot_general | solution.py:45
  487.1 2.9 copy.19
  490.0 9.1 %all_to_all.23 = bf16[2,2048,640]{1,2,0:T(8,128)(2,1)} all-to-all(bf16[2,2048,640]{1,2,0:T(8,128)(2,1)S(1)} %bitcast.27), channel_id=1, replica_groups=mesh['grp'=4,'ep'=32,'tp'=2] {'tp'}, dimensions={0} | all-to-all | bytes 10485760 | tf_op jit(solution)/shard_map/all_to_all | solution.py:16
  499.0 6.0 reduce_sum.22
  505.1 5.1 all_to_all.16
  510.2 0.0 copy-start.1
  510.2 0.0 copy-start.2
  510.2 22.0 %all-to-all-start.2 = ((bf16[2048,32,20]{0,2,1:T(8,128)(2,1)}), bf16[2048,32,20]{0,2,1:T(8,128)(2,1)}, u32[]{:S(2)}, u32[]{:S(2)}) async-start(bf16[2048,32,20]{0,2,1:T(8,128)(2,1)} %all_to_all.16), calls=%async_computation.2 | async-start | bytes 6291456 | tf_op jit(solution)/shard_map/all_to_all | solution.py:52
  532.2 0.0 copy-done.1
  532.2 0.1 copy.11
  532.3 0.1 eq.15
  532.4 0.0 copy-done.2
  532.4 0.1 copy.12
  532.5 0.1 squeeze.13
  532.7 284.1 %all-to-all-done.2 = bf16[2048,32,20]{0,2,1:T(8,128)(2,1)} async-done(((bf16[2048,32,20]{0,2,1:T(8,128)(2,1)}), bf16[2048,32,20]{0,2,1:T(8,128)(2,1)}, u32[]{:S(2)}, u32[]{:S(2)}) %all-to-all-start.2) | async-done | bytes 2621472 | tf_op jit(solution)/shard_map/all_to_all | solution.py:52
  816.8 5.2 all_to_all.18
  822.0 3.1 convolution_convert_fusion.1
  (3 shorter events, 0.0 us)
Async XLA Ops:
  6.5 468.9 %copy-start = (bf16[1,384,4096]{2,1,0:T(8,128)(2,1)S(1)}, bf16[1,384,4096]{2,1,0:T(8,128)(2,1)}, u32[]{:S(2)}) copy-start(bf16[1,384,4096]{2,1,0:T(8,128)(2,1)} %param.11) | copy-start | bytes 9437188
  6.6 445.7 %all-gather.2.cloned.1.call-start = ((), (), s32[]{:S(2)}) async-start(), calls=%async_computation.3 | async-start | bytes 7864320 | tf_op jit(solution)/shard_map/all_gather | solution.py:38
  510.2 22.0 %copy-start.1 = (s32[1,32,20]{1,0,2:T(1,128)S(1)}, s32[1,32,20]{1,0,2:T(1,128)}, u32[]{:S(2)}) copy-start(s32[1,32,20]{1,0,2:T(1,128)} %param.12) | copy-start | bytes 7684
  510.2 22.2 %copy-start.2 = (f32[1,32,20]{1,0,2:T(1,128)S(1)}, f32[1,32,20]{1,0,2:T(1,128)}, u32[]{:S(2)}) copy-start(f32[1,32,20]{1,0,2:T(1,128)} %param.13) | copy-start | bytes 7684
  510.2 306.6 %all-to-all-start.2 = ((bf16[2048,32,20]{0,2,1:T(8,128)(2,1)}), bf16[2048,32,20]{0,2,1:T(8,128)(2,1)}, u32[]{:S(2)}, u32[]{:S(2)}) async-start(bf16[2048,32,20]{0,2,1:T(8,128)(2,1)} %all_to_all.16), calls=%async_computation.2 | async-start | bytes 6291456 | tf_op jit(solution)/shard_map/all_to_all | solution.py:52
Sparse Core Ops, SparseCore 0:
  425.7 26.4 all-gather.1
where the time goes:
time: 833 us; the launch traced here: 832 us
  blocking collectives  406 us (49%)
  waiting for transfers between devices  311 us (37%)
  local copies, waits for them, and re-layouts  47.6 us (6%)
  matrix products  22.1 us (3%)
  starting transfers between devices  22 us (3%)
  between operations  13.5 us (2%)
  other arithmetic  10.1 us (1%)
    all_to_all x1, blocking collectives, shards(): lax.all_to_all(outgoing, 'ep', split_axis=0, concat_axis=0, tiled=True)  397 us
    all_to_all x1, waiting for transfers between devices, shards(): lax.all_to_all(expert_out, 'ep', split_axis=1, concat_axis=1, tiled=True)  284 us
    all_gather x1, waiting for transfers between devices, shards(): arrived = lax.all_gather(landed, 'tp', axis=1, tiled=True)  26.6 us
    all_to_all x1, starting transfers between devices, shards(): lax.all_to_all(expert_out, 'ep', split_axis=1, concat_axis=1, tiled=True)  22 us
  transfers between devices with their start and end apart: 2, of which 2 were waited for; matrix products, arithmetic and copies ran while one was open for 0% of the time, Pallas kernels for 0%

commit v1 on v0

--- a/solution.py
+++ b/solution.py
@@ -35,7 +35,9 @@
     )
     outgoing = jnp.take(source, own_slots, axis=0, mode="clip")
     landed = lax.all_to_all(outgoing, "ep", split_axis=0, concat_axis=0, tiled=True)
-    arrived = lax.all_gather(landed, "tp", axis=1, tiled=True)
+    arrived = jnp.concatenate(
+        lax.all_to_all(jnp.stack([landed] * lax.axis_size("tp")), "tp", 0, 0), axis=1
+    )
     arrived_rows = arrived.reshape(-1, model_width)
     gate_proj = jnp.dot(arrived_rows, gate_weight[0], preferred_element_type=jnp.float32)
     up_value = jnp.dot(arrived_rows, up_weight[0], preferred_element_type=jnp.float32)

time: 833 us -> 804 us (0.965)
  waiting for transfers between devices: 311 us -> 284 us
  blocking collectives: 406 us -> 420 us
  starting transfers between devices: 22 us -> 8.08 us
  between operations: 13.5 us -> 0.07 us
    all_gather x1 -> x0, waiting for transfers between devices: 26.6 us -> none  [shards(): arrived = lax.all_gather(landed, 'tp', axis=1, tiled=True)]
    another operation x0 -> x2, local copies, waits for them, and re-layouts: none -> 14.9 us  [the longest x1 8.6 us: shards(): arrived_rows = arrived.reshape(-1, model_width)]
    all_to_all x0 -> x1, blocking collectives: none -> 14 us  [shards(): lax.all_to_all(jnp.stack([landed] * lax.axis_size('tp')), 'tp', 0, 0)]
    all_to_all x1, starting transfers between devices: 22 us -> 8.08 us  [shards(): lax.all_to_all(expert_out, 'ep', split_axis=1, concat_axis=1, tiled=True)]
  transfers between devices with their start and end apart: 2 -> 1, of which waited for: 2 -> 1; matrix products, arithmetic and copies ran while one was open for 0% -> 0% of each run, Pallas kernels for 0% -> 0%
where the time goes in v1:
time: 804 us; the launch traced here: 803 us
  blocking collectives  420 us (52%)
  waiting for transfers between devices  284 us (35%)
  local copies, waits for them, and re-layouts  50 us (6%)
  matrix products  22 us (3%)
  other arithmetic  17.9 us (2%)
  starting transfers between devices  8.08 us (1%)
    all_to_all x1, blocking collectives, shards(): lax.all_to_all(outgoing, 'ep', split_axis=0, concat_axis=0, tiled=True)  397 us
    all_to_all x1, waiting for transfers between devices, shards(): lax.all_to_all(expert_out, 'ep', split_axis=1, concat_axis=1, tiled=True)  284 us
  transfers between devices with their start and end apart: 1, of which 1 were waited for; matrix products, arithmetic and copies ran while one was open for 0% of the time, Pallas kernels for 0%

profile of v1, /device:TPU:357, one launch (start us, length us, event | category | flops | bytes accessed | tf_op | source)
XLA Modules:
  0.0 802.5 jit_solution(9883864023244133956)
XLA Ops:
  0.0 0.0 copy-start
  0.0 0.8 constant_dynamic-slice_fusion
  0.8 0.1 copy.14
  0.9 0.1 reshape.35
  1.1 1.5 fusion.5
  2.6 2.5 fusion.7
  5.1 9.4 %gather_fusion = bf16[320,4096]{1,0:T(8,128)(2,1)} fusion(bf16[128,4096]{1,0:T(8,128)(2,1)} %fusion.7, s32[1024]{0:T(1024)S(1)} %pad_clamp_fusion), kind=kCustom, calls=%fused_computation | custom fusion | bytes 5244160 | tf_op jit(solution)/shard_map/jit(_take)/gather | solution.py:36
  14.6 4.6 reshape.34
  19.2 397.4 %all_to_all.27 = bf16[32,10,4096]{2,1,0:T(8,128)(2,1)} all-to-all(bf16[32,10,4096]{2,1,0:T(8,128)(2,1)} %reshape.34), channel_id=1, replica_groups=mesh['grp'=4,'ep'=32,'tp'=2] {'ep'}, dimensions={0} | all-to-all | bytes 5242880 | tf_op jit(solution)/shard_map/all_to_all | solution.py:37
  416.6 7.8 pad_maximum_fusion
  424.4 6.2 copy.15
  430.6 14.0 %all_to_all.28 = bf16[2,32,10,4096]{3,1,2,0:T(8,128)(2,1)S(1)} all-to-all(bf16[2,32,10,4096]{3,1,2,0:T(8,128)(2,1)S(1)} %copy.15), channel_id=1, replica_groups=mesh['grp'=4,'ep'=32,'tp'=2] {'tp'}, dimensions={0} | all-to-all | bytes 10485760 | tf_op jit(solution)/shard_map/all_to_all | solution.py:39
  444.6 6.4 copy.16
  451.0 8.6 %reshape_reshape.3 = bf16[640,4096]{1,0:T(8,128)(2,1)} reshape(bf16[32,2,10,4096]{3,2,1,0:T(8,128)(2,1)} %copy.16) | data formatting | bytes 10485760 | tf_op jit(solution)/shard_map/reshape;reshape | solution.py:41
  459.6 7.3 fusion.3
  466.9 0.0 copy-done
  466.9 11.5 %convolution_convert_fusion = bf16[640,4096]{1,0:T(8,128)(2,1)} fusion(bf16[1,384,4096]{2,1,0:T(8,128)(2,1)S(1)} %copy-done, bf16[640,4096]{1,0:T(8,128)(2,1)} %reshape_reshape.3, bf16[1,4096,384]{2,1,0:T(8,128)(2,1)} %param.10, f32[640,384]{1,0:T(8,128)} %fusion.3), kind=kOutput, calls=%fused_computation.2 | convolution fusion | flops 4030627840 | bytes 17760256 | tf_op jit(solution)/shard_map/dot_general | solution.py:47
  478.5 2.9 copy.20
  481.4 9.0 %all_to_all.29 = bf16[2,2048,640]{1,2,0:T(8,128)(2,1)} all-to-all(bf16[2,2048,640]{1,2,0:T(8,128)(2,1)S(1)} %bitcast.30), channel_id=1, replica_groups=mesh['grp'=4,'ep'=32,'tp'=2] {'tp'}, dimensions={0} | all-to-all | bytes 10485760 | tf_op jit(solution)/shard_map/all_to_all | solution.py:16
  490.4 6.0 reduce_sum.22
  496.4 5.2 all_to_all.20
  501.6 0.0 copy-start.1
  501.6 0.0 copy-start.2
  501.6 8.1 %all-to-all-start.3 = ((bf16[2048,32,20]{0,2,1:T(8,128)(2,1)}), bf16[2048,32,20]{0,2,1:T(8,128)(2,1)}, u32[]{:S(2)}, u32[]{:S(2)}) async-start(bf16[2048,32,20]{0,2,1:T(8,128)(2,1)} %all_to_all.20), calls=%async_computation.3 | async-start | bytes 6291456 | tf_op jit(solution)/shard_map/all_to_all | solution.py:54
  509.7 0.0 copy-done.1
  509.7 0.1 copy.12
  509.8 0.1 eq.15
  509.9 0.0 copy-done.2
  509.9 0.1 copy.13
  510.0 0.1 squeeze.13
  510.1 284.1 %all-to-all-done.3 = bf16[2048,32,20]{0,2,1:T(8,128)(2,1)} async-done(((bf16[2048,32,20]{0,2,1:T(8,128)(2,1)}), bf16[2048,32,20]{0,2,1:T(8,128)(2,1)}, u32[]{:S(2)}, u32[]{:S(2)}) %all-to-all-start.3) | async-done | bytes 2621472 | tf_op jit(solution)/shard_map/all_to_all | solution.py:54
  794.2 5.2 all_to_all.22
  799.4 3.1 convolution_convert_fusion.1
  (3 shorter events, 0.0 us)
Async XLA Ops:
  0.0 466.9 %copy-start = (bf16[1,384,4096]{2,1,0:T(8,128)(2,1)S(1)}, bf16[1,384,4096]{2,1,0:T(8,128)(2,1)}, u32[]{:S(2)}) copy-start(bf16[1,384,4096]{2,1,0:T(8,128)(2,1)} %param.11) | copy-start | bytes 9437188
  501.6 8.1 %copy-start.1 = (s32[1,32,20]{1,0,2:T(1,128)S(1)}, s32[1,32,20]{1,0,2:T(1,128)}, u32[]{:S(2)}) copy-start(s32[1,32,20]{1,0,2:T(1,128)} %param.12) | copy-start | bytes 7684
  501.6 8.3 %copy-start.2 = (f32[1,32,20]{1,0,2:T(1,128)S(1)}, f32[1,32,20]{1,0,2:T(1,128)}, u32[]{:S(2)}) copy-start(f32[1,32,20]{1,0,2:T(1,128)} %param.13) | copy-start | bytes 7684
  501.6 292.7 %all-to-all-start.3 = ((bf16[2048,32,20]{0,2,1:T(8,128)(2,1)}), bf16[2048,32,20]{0,2,1:T(8,128)(2,1)}, u32[]{:S(2)}, u32[]{:S(2)}) async-start(bf16[2048,32,20]{0,2,1:T(8,128)(2,1)} %all_to_all.20), calls=%async_computation.3 | async-start | bytes 6291456 | tf_op jit(solution)/shard_map/all_to_all | solution.py:54
